TPU v7x, 32 devices: a whole 2x2x4 slice. The times are simulated.
32 devices in a mesh: sp: 8 (over z, y), tp: 4 (over x, core).
Axes of the slice: x: 2, y: 2, z: 4, core: 2. Of those that a mesh axis runs over, the one named last changes fastest.
Arguments:
- stream: bfloat16 [4096, 2048], P('sp', 'tp'), may hold values from -6 to 6
- doc_ids: int32 [4096], P('sp'), may hold values from 0 to 3, never falling along the last dimension, each value on 1 to 2304 neighbouring positions
- norm_gain: float32 [2, 2048], replicated, may hold values from 0.1 to 1.9
- gate_proj: bfloat16 [2, 2048, 2048], P(None, 'sp', 'tp'), may hold values from -0.125 to 0.125
- input_gate: bfloat16 [2, 2048, 2048], P(None, 'sp', 'tp'), may hold values from -0.125 to 0.125
- value_proj: bfloat16 [2, 2048, 2048], P(None, 'sp', 'tp'), may hold values from -0.125 to 0.125
- taps: float32 [2, 3, 2048], P(None, None, 'tp'), may hold values from -3 to 3
- out_proj: bfloat16 [2, 2048, 2048], P(None, 'tp', 'sp'), may hold values from -0.125 to 0.125
Outputs:
- result: bfloat16 [4096, 2048], P('sp', 'tp')
Inputs may be any that keep to these rules, and one draw needn't show every extreme that they name: `doc_ids`: document numbers never fall along the sequence; each document holds 1 to 2304 positions.
All inputs are finite; a program needn't handle non-finite values.
Results may differ from a plain program's by a relative error of at most 0.03.
Values may be sent and summed in bfloat16 or wider, within the bound.
A program may use at most 64 MiB of HBM per device.

v0:
```python
import jax
import jax.numpy as jnp
from jax import lax
from jax.sharding import PartitionSpec as P

epsilon = 1e-06


def with_halo(value, sides, width):
    for axis, dim in sides:
        size, length = (lax.axis_size(axis), value.shape[dim])
        up = [(i, (i + 1) % size) for i in range(size - 1)]
        down = [(j, i) for i, j in up]
        last = lax.slice_in_dim(value, length - width, length, axis=dim)
        leading = lax.slice_in_dim(value, 0, width, axis=dim)
        before = lax.ppermute(last, axis, up)
        after = lax.ppermute(leading, axis, down)
        value = jnp.concatenate([before, value, after], axis=dim)
    return value


def per_device(stream, doc_ids, norm_gain, gate_proj, input_gate, value_proj, taps, out_proj):
    layers = gate_proj.shape[0]
    gathered_in = (
        lax.all_gather(gate_proj, "sp", axis=1, tiled=True),
        lax.all_gather(input_gate, "sp", axis=1, tiled=True),
        lax.all_gather(value_proj, "sp", axis=1, tiled=True),
    )
    gathered_out = lax.all_gather(out_proj, "sp", axis=2, tiled=True)
    current = stream
    for layer_index in range(layers):
        full_rows = lax.all_gather(current, "tp", axis=1, tiled=True)
        widened = full_rows.astype(jnp.float32)
        scale = lax.rsqrt(jnp.mean(widened * widened, axis=-1, keepdims=True) + epsilon)
        normed = (widened * scale * norm_gain[layer_index]).astype(jnp.bfloat16)
        gate_b = jnp.dot(normed, gathered_in[0][layer_index], preferred_element_type=jnp.float32)
        gate_c = jnp.dot(normed, gathered_in[1][layer_index], preferred_element_type=jnp.float32)
        values = jnp.dot(normed, gathered_in[2][layer_index], preferred_element_type=jnp.float32)
        gate_b = gate_b.astype(jnp.bfloat16)
        gate_c = gate_c.astype(jnp.bfloat16)
        values = values.astype(jnp.bfloat16)
        mixed_in = (gate_c.astype(jnp.float32) * values.astype(jnp.float32)).astype(jnp.bfloat16)
        padded, doc_padded = (
            with_halo(mixed_in, (("sp", 0),), 1),
            with_halo(doc_ids, (("sp", 0),), 1),
        )
        same_prev = (doc_padded[:-2] == doc_ids)[:, None]
        same_next = (doc_padded[2:] == doc_ids)[:, None]
        kernel_taps = taps[layer_index]
        convolved = (
            jnp.where(same_prev, kernel_taps[0] * padded[:-2].astype(jnp.float32), 0.0)
            + kernel_taps[1] * mixed_in.astype(jnp.float32)
            + jnp.where(same_next, kernel_taps[2] * padded[2:].astype(jnp.float32), 0.0)
        )
        gated = (gate_b.astype(jnp.float32) * convolved).astype(jnp.bfloat16)
        partials = jnp.dot(gated, gathered_out[layer_index], preferred_element_type=jnp.float32)
        summed = lax.psum_scatter(
            partials.astype(jnp.bfloat16), "tp", scatter_dimension=1, tiled=True
        ).astype(jnp.float32)
        current = (current.astype(jnp.float32) + summed).astype(jnp.bfloat16)
    return current


def solution(mesh):
    in_specs = (
        P("sp", "tp"),
        P("sp"),
        P(),
        P(None, "sp", "tp"),
        P(None, "sp", "tp"),
        P(None, "sp", "tp"),
        P(None, None, "tp"),
        P(None, "tp", "sp"),
    )
    out_specs = P("sp", "tp")
    return jax.shard_map(
        per_device, mesh=mesh, in_specs=in_specs, out_specs=out_specs, check_vma=False
    )
```

profile of v0, /device:TPU:0, one launch (start us, length us, event | category | flops | bytes accessed | tf_op | source)
XLA Modules:
  0.0 454.6 jit_solution(15519410524372381653)
XLA Ops:
  6.5 0.0 all-gather.7.cloned.1.call-start
  6.5 0.7 all-gather.7.cloned.1.call-update
  7.3 0.0 all-gather.13.cloned.1.call-start
  7.3 0.7 all-gather.13.cloned.1.call-update
  8.0 0.0 all-gather.11.cloned.1.call-start
  8.1 0.7 all-gather.11.cloned.1.call-update
  8.7 0.0 all-gather.9.cloned.1.call-start
  8.8 0.5 all-gather.9.cloned.1.call-update
  9.3 0.0 all-gather.15.cloned.1.call-start
  9.4 0.5 all-gather.15.cloned.1.call-update
  9.9 0.0 reduce-scatter.3.cloned.1.call-start
  9.9 1.3 fusion.64
  11.3 5.4 %collective-permute-start = (s32[1]{0:T(128)}, s32[1]{0:T(128)}, u32[]{:S(2)}, u32[]{:S(2)}) collective-permute-start(s32[1]{0:T(128)} %get-tuple-element.21), channel_id=1, source_target_pairs={{0,4},{4,8},{8,12},{12,16},{16,20},{20,24},{24,28},{1,5},{5,9},{9,... | collective-permute-start | bytes 20 | tf_op jit(solution)/shard_map/ppermute | solution.py:16
  16.7 1.3 collective-permute-start.2
  18.0 0.8 fusion.63
  18.8 0.8 fusion.62
  19.6 0.0 collective-permute-done
  19.6 2.5 collective-permute-done.2
  22.2 2.1 pad_add_fusion
  24.3 9.9 %all-gather.7.cloned.1.call-done = bf16[512,2048]{1,0:T(8,128)(2,1)} async-done(((bf16[512,512]{1,0:T(8,128)(2,1)}), bf16[512,2048]{1,0:T(8,128)(2,1)}) %all-gather.7.cloned.1.call-update) | async-done | bytes 2097168 | tf_op jit(solution)/shard_map/all_gather | solution.py:32
  34.2 2.1 fusion
  36.3 72.9 %all-gather.13.cloned.1.call-done = bf16[2,2048,512]{2,1,0:T(8,128)(2,1)} async-done(((bf16[2,256,512]{2,1,0:T(8,128)(2,1)}), bf16[2,2048,512]{2,1,0:T(8,128)(2,1)}) %all-gather.13.cloned.1.call-update) | async-done | bytes 4194320 | tf_op jit(solution)/shard_map/all_gather | solution.py:27
  109.2 0.0 copy-start.2
  109.2 4.7 %fusion.19 = f32[512,512]{1,0:T(8,128)} fusion(bf16[2,2048,512]{2,1,0:T(8,128)(2,1)} %all-gather.13.cloned.1.call-done, bf16[512,2048]{1,0:T(8,128)(2,1)} %all-gather.7.cloned.1.call-done, f32[2048]{0:T(1024)S(1)} %bitcast.79, f32[512]{0:T(512)S(1)} %add_rsqrt_fusion.1), kind=kOutput, calls=%fused_computation.33 | convolution fusion | flops 1078460416 | bytes 5253120 | tf_op jit(solution)/shard_map/dot_general | solution.py:38
  113.9 0.0 copy-start.4
  113.9 68.9 %all-gather.11.cloned.1.call-done = bf16[2,2048,512]{2,1,0:T(8,128)(2,1)} async-done(((bf16[2,256,512]{2,1,0:T(8,128)(2,1)}), bf16[2,2048,512]{2,1,0:T(8,128)(2,1)}) %all-gather.11.cloned.1.call-update) | async-done | bytes 4194320 | tf_op jit(solution)/shard_map/all_gather | solution.py:26
  182.7 0.0 copy-done.2
  182.7 3.1 fusion.30
  185.9 2.5 collective-permute-start.1
  188.4 1.3 collective-permute-start.3
  189.7 0.0 copy-done.4
  189.7 0.1 slice_compare_fusion.1
  189.8 66.4 %all-gather.9.cloned.1.call-done = bf16[2,2048,512]{2,1,0:T(8,128)(2,1)} async-done(((bf16[2,256,512]{2,1,0:T(8,128)(2,1)}), bf16[2,2048,512]{2,1,0:T(8,128)(2,1)}) %all-gather.9.cloned.1.call-update) | async-done | bytes 4194320 | tf_op jit(solution)/shard_map/all_gather | solution.py:25
  256.1 75.1 %all-gather.15.cloned.1.call-done = bf16[2,512,2048]{2,1,0:T(8,128)(2,1)} async-done(((bf16[2,512,256]{2,1,0:T(8,128)(2,1)}), bf16[2,512,2048]{2,1,0:T(8,128)(2,1)}) %all-gather.15.cloned.1.call-update) | async-done | bytes 4194320 | tf_op jit(solution)/shard_map/all_gather | solution.py:29
  331.2 0.0 collective-permute-done.1
  331.2 0.0 collective-permute-done.3
  331.2 0.0 copy-start.1
  331.2 6.3 %convolution_convert_fusion.1 = bf16[512,2048]{1,0:T(8,128)(2,1)} fusion(bf16[2,512,2048]{2,1,0:T(8,128)(2,1)} %all-gather.15.cloned.1.call-done, bf16[2,2048,512]{2,1,0:T(8,128)(2,1)} %all-gather.9.cloned.1.call-done, bf16[512,512]{1,0:T(8,128)(2,1)S(1)} %fusion.30, bf16[1,512]{1,0:T(2,128)(2,1)S(1)} %collective-permute-done.3, ...), kind=kOutput, calls=%fused_computation.11 | convolution fusion | flops 2157969408 | bytes 8932352 | tf_op jit(solution)/shard_map/dot_general | solution.py:56
  337.5 0.0 reduce-scatter.3.cloned.1.call-update
  337.6 0.0 all-gather.17.cloned.1.call-start
  337.6 29.4 %reduce-scatter.3.cloned.1.call-done = bf16[512,512]{1,0:T(8,128)(2,1)} async-done(((bf16[512,2048]{1,0:T(8,128)(2,1)}), bf16[512,512]{1,0:T(8,128)(2,1)}) %reduce-scatter.3.cloned.1.call-update) | async-done | bytes 524304 | tf_op jit(solution)/shard_map/reduce_scatter | solution.py:57
  367.0 0.0 copy-done.1
  367.1 2.0 add_convert_fusion.1
  369.0 0.0 all-gather.17.cloned.1.call-update
  369.0 0.0 reduce-scatter.5.cloned.1.call-start
  369.1 22.7 %all-gather.17.cloned.1.call-done = bf16[512,2048]{1,0:T(8,128)(2,1)} async-done(((bf16[512,512]{1,0:T(8,128)(2,1)}), bf16[512,2048]{1,0:T(8,128)(2,1)}) %all-gather.17.cloned.1.call-update) | async-done | bytes 2097168 | tf_op jit(solution)/shard_map/all_gather | solution.py:32
  391.8 2.1 fusion.3
  393.8 0.0 copy-start.3
  393.8 0.0 copy-start.5
  393.9 3.7 fusion.27
  397.5 0.0 copy-done.3
  397.5 0.4 copy-done.5
  397.9 1.3 fusion.28
  399.2 3.4 collective-permute-start.4
  402.6 1.3 collective-permute-start.5
  403.9 0.0 collective-permute-done.4
  403.9 4.2 collective-permute-done.5
  408.1 0.0 copy-start
  408.1 6.3 %convolution_convert_fusion = bf16[512,2048]{1,0:T(8,128)(2,1)} fusion(bf16[2,512,2048]{2,1,0:T(8,128)(2,1)} %all-gather.15.cloned.1.call-done, bf16[2,2048,512]{2,1,0:T(8,128)(2,1)} %all-gather.9.cloned.1.call-done, bf16[512,512]{1,0:T(8,128)(2,1)S(1)} %fusion.28, bf16[1,512]{1,0:T(2,128)(2,1)S(1)} %collective-permute-done.5, ...), kind=kOutput, calls=%fused_computation.10 | convolution fusion | flops 2157969408 | bytes 8932352 | tf_op jit(solution)/shard_map/dot_general | solution.py:56
  414.4 0.0 reduce-scatter.5.cloned.1.call-update
  414.5 31.3 %reduce-scatter.5.cloned.1.call-done = bf16[512,512]{1,0:T(8,128)(2,1)} async-done(((bf16[512,2048]{1,0:T(8,128)(2,1)}), bf16[512,512]{1,0:T(8,128)(2,1)}) %reduce-scatter.5.cloned.1.call-update) | async-done | bytes 524304 | tf_op jit(solution)/shard_map/reduce_scatter | solution.py:57
  445.8 0.0 copy-done
  445.8 2.0 add_convert_fusion
  (4 shorter events, 0.0 us)
Async XLA Ops:
  6.5 27.7 %all-gather.7.cloned.1.call-start = ((), (), s32[]{:S(2)}) async-start(), calls=%async_computation.2 | async-start | bytes 2621440 | tf_op jit(solution)/shard_map/all_gather | solution.py:32
  7.3 101.9 %all-gather.13.cloned.1.call-start = ((), (), s32[]{:S(2)}) async-start(), calls=%async_computation.5 | async-start | bytes 4718592 | tf_op jit(solution)/shard_map/all_gather | solution.py:27
  8.0 174.7 %all-gather.11.cloned.1.call-start = ((), (), s32[]{:S(2)}) async-start(), calls=%async_computation.4 | async-start | bytes 4718592 | tf_op jit(solution)/shard_map/all_gather | solution.py:26
  8.7 247.4 %all-gather.9.cloned.1.call-start = ((), (), s32[]{:S(2)}) async-start(), calls=%async_computation.3 | async-start | bytes 4718592 | tf_op jit(solution)/shard_map/all_gather | solution.py:25
  9.3 321.9 %all-gather.15.cloned.1.call-start = ((), (), s32[]{:S(2)}) async-start(), calls=%async_computation.6 | async-start | bytes 4718592 | tf_op jit(solution)/shard_map/all_gather | solution.py:29
  9.9 357.1 %reduce-scatter.3.cloned.1.call-start = ((), (), s32[]{:S(2)}) async-start(), calls=%async_computation.7 | async-start | bytes 2621440 | tf_op jit(solution)/shard_map/reduce_scatter | solution.py:57
  11.3 8.3 %collective-permute-start = (s32[1]{0:T(128)}, s32[1]{0:T(128)}, u32[]{:S(2)}, u32[]{:S(2)}) collective-permute-start(s32[1]{0:T(128)} %get-tuple-element.21), channel_id=1, source_target_pairs={{0,4},{4,8},{8,12},{12,16},{16,20},{20,24},{24,28},{1,5},{5,9},{9,... | collective-permute-start | bytes 20 | tf_op jit(solution)/shard_map/ppermute | solution.py:16
  16.7 5.5 %collective-permute-start.2 = (s32[1]{0:T(128)}, s32[1]{0:T(128)}, u32[]{:S(2)}, u32[]{:S(2)}) collective-permute-start(s32[1]{0:T(128)} %get-tuple-element.22), channel_id=1, source_target_pairs={{4,0},{8,4},{12,8},{16,12},{20,16},{24,20},{28,24},{5,1},{9,5},{13... | collective-permute-start | bytes 20 | tf_op jit(solution)/shard_map/ppermute | solution.py:17
  109.2 73.5 %copy-start.2 = (bf16[512,2048]{1,0:T(8,128)(2,1)S(1)}, bf16[512,2048]{1,0:T(8,128)(2,1)}, u32[]{:S(2)}) copy-start(bf16[512,2048]{1,0:T(8,128)(2,1)} %all-gather.7.cloned.1.call-done) | copy-start | bytes 6291460
  113.9 75.8 %copy-start.4 = (s32[512]{0:T(512)S(1)}, s32[512]{0:T(512)}, u32[]{:S(2)}) copy-start(s32[512]{0:T(512)} %param.9) | copy-start | bytes 6148
  185.9 145.3 %collective-permute-start.1 = (bf16[1,512]{1,0:T(2,128)(2,1)S(1)}, bf16[1,512]{1,0:T(2,128)(2,1)S(1)}, u32[]{:S(2)}, u32[]{:S(2)}) collective-permute-start(bf16[1,512]{1,0:T(2,128)(2,1)S(1)} %get-tuple-element.7), channel_id=1, source_target_pairs={{0,4},{4,8},{8,12},{12,16},{16,20},{20,24},{24,28},{1,5},{5,9},{9,... | collective-permute-start | bytes 3080 | tf_op jit(solution)/shard_map/ppermute | solution.py:16
  188.4 142.8 %collective-permute-start.3 = (bf16[1,512]{1,0:T(2,128)(2,1)S(1)}, bf16[1,512]{1,0:T(2,128)(2,1)S(1)}, u32[]{:S(2)}, u32[]{:S(2)}) collective-permute-start(bf16[1,512]{1,0:T(2,128)(2,1)S(1)} %get-tuple-element.8), channel_id=1, source_target_pairs={{4,0},{8,4},{12,8},{16,12},{20,16},{24,20},{28,24},{5,1},{9,5},{13... | collective-permute-start | bytes 3080 | tf_op jit(solution)/shard_map/ppermute | solution.py:17
  331.2 35.8 %copy-start.1 = (bf16[512,512]{1,0:T(8,128)(2,1)S(1)}, bf16[512,512]{1,0:T(8,128)(2,1)}, u32[]{:S(2)}) copy-start(bf16[512,512]{1,0:T(8,128)(2,1)} %param.8) | copy-start | bytes 1572868
  337.6 54.2 %all-gather.17.cloned.1.call-start = ((), (), s32[]{:S(2)}) async-start(), calls=%async_computation.8 | async-start | bytes 2621440 | tf_op jit(solution)/shard_map/all_gather | solution.py:32
  369.0 76.7 %reduce-scatter.5.cloned.1.call-start = ((), (), s32[]{:S(2)}) async-start(), calls=%async_computation.9 | async-start | bytes 2621440 | tf_op jit(solution)/shard_map/reduce_scatter | solution.py:57
  393.8 3.7 copy-start.3
  393.8 4.1 copy-start.5
  399.2 4.7 %collective-permute-start.4 = (bf16[1,512]{1,0:T(2,128)(2,1)S(1)}, bf16[1,512]{1,0:T(2,128)(2,1)S(1)}, u32[]{:S(2)}, u32[]{:S(2)}) collective-permute-start(bf16[1,512]{1,0:T(2,128)(2,1)S(1)} %get-tuple-element.5), channel_id=1, source_target_pairs={{0,4},{4,8},{8,12},{12,16},{16,20},{20,24},{24,28},{1,5},{5,9},{9,... | collective-permute-start | bytes 3080 | tf_op jit(solution)/shard_map/ppermute | solution.py:16
  402.6 5.5 %collective-permute-start.5 = (bf16[1,512]{1,0:T(2,128)(2,1)S(1)}, bf16[1,512]{1,0:T(2,128)(2,1)S(1)}, u32[]{:S(2)}, u32[]{:S(2)}) collective-permute-start(bf16[1,512]{1,0:T(2,128)(2,1)S(1)} %get-tuple-element.6), channel_id=1, source_target_pairs={{4,0},{8,4},{12,8},{16,12},{20,16},{24,20},{28,24},{5,1},{9,5},{13... | collective-permute-start | bytes 3080 | tf_op jit(solution)/shard_map/ppermute | solution.py:17
  408.1 37.7 %copy-start = (bf16[512,512]{1,0:T(8,128)(2,1)S(1)}, bf16[512,512]{1,0:T(8,128)(2,1)}, u32[]{:S(2)}) copy-start(bf16[512,512]{1,0:T(8,128)(2,1)} %add_convert_fusion.1) | copy-start | bytes 1572868
Sparse Core Ops, SparseCore 0:
  8.9 25.2 all-gather.6
  36.4 72.7 all-gather.12
  111.4 71.2 all-gather.10
  184.8 71.2 all-gather.8
  258.0 73.1 all-gather.14
  337.7 29.3 reduce-scatter.2
  369.2 22.5 all-gather.16
  414.6 31.1 reduce-scatter.4
where the time goes:
time: 455 us
  waiting for transfers between devices  386 us (85%)
  matrix products  25.4 us (6%)
  starting transfers between devices  15.4 us (3%)
  between operations  13.6 us (3%)
  other arithmetic  10.3 us (2%)
    all_gather x1, waiting for transfers between devices, per_device(): gathered_out = lax.all_gather(out_proj, 'sp', axis=2, tiled=True)  75.1 us
    all_gather x1, waiting for transfers between devices, per_device(): lax.all_gather(value_proj, 'sp', axis=1, tiled=True)  72.9 us
    all_gather x1, waiting for transfers between devices, per_device(): lax.all_gather(input_gate, 'sp', axis=1, tiled=True)  68.9 us
    all_gather x1, waiting for transfers between devices, per_device(): lax.all_gather(gate_proj, 'sp', axis=1, tiled=True)  66.4 us
    reduce_scatter x2, waiting for transfers between devices, per_device(): lax.psum_scatter(partials.astype(jnp.bfloat16), 'tp', scatter_dimension=1...  60.7 us
    all_gather x2, waiting for transfers between devices, per_device(): full_rows = lax.all_gather(current, 'tp', axis=1, tiled=True)  32.6 us
    dot_general x2, matrix products, per_device(): jnp.dot(gated, gathered_out[layer_index], preferred_element_type=jnp.floa...  12.7 us
    ppermute x3, starting transfers between devices, with_halo(): before = lax.ppermute(last, axis, up)  11.2 us
  transfers between devices with their start and end apart: 14, of which 10 were waited for; matrix products, arithmetic and copies ran while one was open for 3% of the time, Pallas kernels for 0%

commit v1 on v0

--- a/solution.py
+++ b/solution.py
@@ -26,7 +26,16 @@
         lax.all_gather(input_gate, "sp", axis=1, tiled=True),
         lax.all_gather(value_proj, "sp", axis=1, tiled=True),
     )
-    gathered_out = lax.all_gather(out_proj, "sp", axis=2, tiled=True)
+    ways = lax.axis_size("sp")
+    up_2 = [(d, (d + 1) % ways) for d in range(ways)]
+    down_2 = [(d, (d - 1) % ways) for d in range(ways)]
+    earlier, later = ([out_proj], [out_proj])
+    for _ in range(ways // 2):
+        earlier.append(lax.ppermute(earlier[-1], "sp", up_2))
+    for _ in range((ways - 1) // 2):
+        later.append(lax.ppermute(later[-1], "sp", down_2))
+    line = jnp.concatenate([*earlier[::-1], *later[1:]], axis=2)
+    gathered_out = jnp.roll(line, (lax.axis_index("sp") - ways // 2) * out_proj.shape[2], axis=2)
     current = stream
     for layer_index in range(layers):
         full_rows = lax.all_gather(current, "tp", axis=1, tiled=True)

time: 455 us -> 413 us (0.908)
  waiting for transfers between devices: 386 us -> 305 us
  starting transfers between devices: 15.4 us -> 39.1 us
  local copies, waits for them, and re-layouts: 3.38 us -> 17.5 us
    all_gather x1 -> x0, waiting for transfers between devices: 75.1 us -> none  [per_device(): gathered_out = lax.all_gather(out_proj, 'sp', axis=2, tiled=True)]
    ppermute x0 -> x7, waiting for transfers between devices: none -> 69.2 us  [the longest x4 47.9 us: per_device(): earlier.append(lax.ppermute(earlier[-1], 'sp', up_2))]
    all_gather x1, waiting for transfers between devices: 72.9 us -> 11 us  [per_device(): lax.all_gather(value_proj, 'sp', axis=1, tiled=True)]
    ppermute x0 -> x7, starting transfers between devices: none -> 26.5 us  [the longest x3 21 us: per_device(): later.append(lax.ppermute(later[-1], 'sp', down_2))]
    unnamed x12 -> x29, local copies, waits for them, and re-layouts: 0.4 us -> 13.6 us
    all_gather x2, waiting for transfers between devices: 32.6 us -> 22.7 us  [per_device(): full_rows = lax.all_gather(current, 'tp', axis=1, tiled=True)]
  transfers between devices with their start and end apart: 14 -> 20, of which waited for: 10 -> 12; matrix products, arithmetic and copies ran while one was open for 3% -> 7% of each run, Pallas kernels for 0% -> 0%
where the time goes in v1:
time: 413 us; the launch traced here: 412 us
  waiting for transfers between devices  305 us (74%)
  starting transfers between devices  39.1 us (9%)
  matrix products  26 us (6%)
  local copies, waits for them, and re-layouts  17.5 us (4%)
  between operations  13.7 us (3%)
  other arithmetic  10.9 us (3%)
    all_gather x1, waiting for transfers between devices, per_device(): lax.all_gather(input_gate, 'sp', axis=1, tiled=True)  69.1 us
    all_gather x1, waiting for transfers between devices, per_device(): lax.all_gather(gate_proj, 'sp', axis=1, tiled=True)  65.5 us
    reduce_scatter x2, waiting for transfers between devices, per_device(): lax.psum_scatter(partials.astype(jnp.bfloat16), 'tp', scatter_dimension=1...  61.1 us
    ppermute x4, waiting for transfers between devices, per_device(): earlier.append(lax.ppermute(earlier[-1], 'sp', up_2))  47.9 us
    all_gather x2, waiting for transfers between devices, per_device(): full_rows = lax.all_gather(current, 'tp', axis=1, tiled=True)  22.7 us
    ppermute x3, waiting for transfers between devices, per_device(): later.append(lax.ppermute(later[-1], 'sp', down_2))  21.3 us
    ppermute x3, starting transfers between devices, per_device(): later.append(lax.ppermute(later[-1], 'sp', down_2))  21 us
    unnamed x29, local copies, waits for them, and re-layouts  13.6 us
  transfers between devices with their start and end apart: 20, of which 12 were waited for; matrix products, arithmetic and copies ran while one was open for 7% of the time, Pallas kernels for 0%

profile of v1, /device:TPU:0, one launch (start us, length us, event | category | flops | bytes accessed | tf_op | source)
XLA Modules:
  0.0 412.4 jit_solution(6019876915247003856)
XLA Ops:
  6.5 0.7 all-gather.6.cloned.1.call-update
  7.3 0.0 all-gather.12.cloned.1.call-start
  7.3 0.7 all-gather.12.cloned.1.call-update
  8.0 0.0 all-gather.10.cloned.1.call-start
  8.1 0.7 all-gather.10.cloned.1.call-update
  8.7 0.0 all-gather.8.cloned.1.call-start
  8.8 0.5 all-gather.8.cloned.1.call-update
  9.4 3.0 collective-permute-start.4
  12.4 15.2 %collective-permute-done.4 = bf16[2,512,256]{2,1,0:T(8,128)(2,1)S(1)} collective-permute-done((bf16[2,512,256]{2,1,0:T(8,128)(2,1)}, bf16[2,512,256]{2,1,0:T(8,128)(2,1)S(1)}, u32[]{:S(2)}, u32[]{:S(2)}) %collective-permute-start.4) | collective-permute-done | bytes 524320 | tf_op jit(solution)/shard_map/ppermute | solution.py:34
  27.6 4.7 %collective-permute-start.8 = (bf16[2,512,256]{2,1,0:T(8,128)(2,1)}, bf16[2,512,256]{2,1,0:T(8,128)(2,1)S(1)}, u32[]{:S(2)}, u32[]{:S(2)}) collective-permute-start(bf16[2,512,256]{2,1,0:T(8,128)(2,1)} %param.15), channel_id=1, source_target_pairs={{0,28},{4,0},{8,4},{12,8},{16,12},{20,16},{24,20},{28,24},{1,29},{... | collective-permute-start | bytes 1572872 | tf_op jit(solution)/shard_map/ppermute | solution.py:36
  32.3 23.5 %collective-permute-done.5 = bf16[2,512,256]{2,1,0:T(8,128)(2,1)S(1)} collective-permute-done((bf16[2,512,256]{2,1,0:T(8,128)(2,1)S(1)}, bf16[2,512,256]{2,1,0:T(8,128)(2,1)S(1)}, u32[]{:S(2)}, u32[]{:S(2)}) %collective-permute-start.5) | collective-permute-done | bytes 524320 | tf_op jit(solution)/shard_map/ppermute | solution.py:34
  55.8 2.5 collective-permute-start.6
  58.3 1.3 fusion.66
  59.6 2.5 collective-permute-start
  62.1 1.3 collective-permute-start.2
  63.4 0.8 fusion.64
  64.2 4.8 %collective-permute-start.9 = (bf16[2,512,256]{2,1,0:T(8,128)(2,1)S(1)}, bf16[2,512,256]{2,1,0:T(8,128)(2,1)S(1)}, u32[]{:S(2)}, u32[]{:S(2)}) collective-permute-start(bf16[2,512,256]{2,1,0:T(8,128)(2,1)S(1)} %collective-permute-done.8), channel_id=1, source_target_pairs={{0,28},{4,0},{8,4},{12,8},{16,12},{20,16},{24,20},{28,24},{1,29},{... | collective-permute-start | bytes 1572872 | tf_op jit(solution)/shard_map/ppermute | solution.py:36
  69.1 9.2 %collective-permute-done.6 = bf16[2,512,256]{2,1,0:T(8,128)(2,1)S(1)} collective-permute-done((bf16[2,512,256]{2,1,0:T(8,128)(2,1)S(1)}, bf16[2,512,256]{2,1,0:T(8,128)(2,1)S(1)}, u32[]{:S(2)}, u32[]{:S(2)}) %collective-permute-start.6) | collective-permute-done | bytes 524320 | tf_op jit(solution)/shard_map/ppermute | solution.py:34
  78.3 0.8 fusion.65
  79.1 2.1 pad_add_fusion
  81.2 0.8 slice_compare_fusion.1
  82.0 14.5 %collective-permute-done.9 = bf16[2,512,256]{2,1,0:T(8,128)(2,1)S(1)} collective-permute-done((bf16[2,512,256]{2,1,0:T(8,128)(2,1)S(1)}, bf16[2,512,256]{2,1,0:T(8,128)(2,1)S(1)}, u32[]{:S(2)}, u32[]{:S(2)}) %collective-permute-start.9) | collective-permute-done | bytes 524320 | tf_op jit(solution)/shard_map/ppermute | solution.py:36
  96.4 11.4 %collective-permute-start.10 = (bf16[2,512,256]{2,1,0:T(8,128)(2,1)S(1)}, bf16[2,512,256]{2,1,0:T(8,128)(2,1)S(1)}, u32[]{:S(2)}, u32[]{:S(2)}) collective-permute-start(bf16[2,512,256]{2,1,0:T(8,128)(2,1)S(1)} %collective-permute-done.9), channel_id=1, source_target_pairs={{0,28},{4,0},{8,4},{12,8},{16,12},{20,16},{24,20},{28,24},{1,29},{... | collective-permute-start | bytes 1572872 | tf_op jit(solution)/shard_map/ppermute | solution.py:36
  107.9 0.9 constant_dynamic-update-slice_fusion.15
  108.8 0.9 constant_dynamic-update-slice_fusion.14
  109.6 0.9 constant_dynamic-update-slice_fusion.13
  110.5 0.9 constant_dynamic-update-slice_fusion.12
  111.4 0.9 constant_dynamic-update-slice_fusion.11
  112.3 0.9 constant_dynamic-update-slice_fusion.10
  113.2 0.9 constant_dynamic-update-slice_fusion.9
  114.0 6.8 %collective-permute-done.10 = bf16[2,512,256]{2,1,0:T(8,128)(2,1)S(1)} collective-permute-done((bf16[2,512,256]{2,1,0:T(8,128)(2,1)S(1)}, bf16[2,512,256]{2,1,0:T(8,128)(2,1)S(1)}, u32[]{:S(2)}, u32[]{:S(2)}) %collective-permute-start.10) | collective-permute-done | bytes 524320 | tf_op jit(solution)/shard_map/ppermute | solution.py:36
  120.8 0.9 constant_dynamic-update-slice_fusion.8
  121.7 0.9 constant_dynamic-update-slice_fusion.7
  122.6 0.9 constant_dynamic-update-slice_fusion.6
  123.5 0.9 constant_dynamic-update-slice_fusion.5
  124.4 0.9 constant_dynamic-update-slice_fusion.4
  125.3 0.9 constant_dynamic-update-slice_fusion.3
  126.2 0.9 constant_dynamic-update-slice_fusion.2
  127.0 0.9 constant_dynamic-update-slice_fusion.1
  127.9 2.1 fusion
  130.0 11.0 %all-gather.12.cloned.1.call-done = bf16[2,2048,512]{2,1,0:T(8,128)(2,1)} async-done(((bf16[2,256,512]{2,1,0:T(8,128)(2,1)}), bf16[2,2048,512]{2,1,0:T(8,128)(2,1)}) %all-gather.12.cloned.1.call-update) | async-done | bytes 4194320 | tf_op jit(solution)/shard_map/all_gather | solution.py:27
  140.9 4.6 %fusion.19 = f32[512,512]{1,0:T(8,128)} fusion(bf16[2,2048,512]{2,1,0:T(8,128)(2,1)} %all-gather.12.cloned.1.call-done, bf16[512,2048]{1,0:T(8,128)(2,1)} %all-gather.6.cloned.1.call-done, f32[2048]{0:T(1024)S(1)} %bitcast.79, f32[512]{0:T(512)S(1)} %add_rsqrt_fusion.1), kind=kOutput, calls=%fused_computation.33 | convolution fusion | flops 1078460416 | bytes 5253120 | tf_op jit(solution)/shard_map/dot_general | solution.py:47
  145.6 69.1 %all-gather.10.cloned.1.call-done = bf16[2,2048,512]{2,1,0:T(8,128)(2,1)} async-done(((bf16[2,256,512]{2,1,0:T(8,128)(2,1)}), bf16[2,2048,512]{2,1,0:T(8,128)(2,1)}) %all-gather.10.cloned.1.call-update) | async-done | bytes 4194320 | tf_op jit(solution)/shard_map/all_gather | solution.py:26
  214.7 3.2 fusion.30
  217.9 2.5 collective-permute-start.1
  220.4 1.3 collective-permute-start.3
  221.7 0.9 constant_dynamic-update-slice_fusion
  222.6 65.5 %all-gather.8.cloned.1.call-done = bf16[2,2048,512]{2,1,0:T(8,128)(2,1)} async-done(((bf16[2,256,512]{2,1,0:T(8,128)(2,1)}), bf16[2,2048,512]{2,1,0:T(8,128)(2,1)}) %all-gather.8.cloned.1.call-update) | async-done | bytes 4194320 | tf_op jit(solution)/shard_map/all_gather | solution.py:25
  288.1 6.9 %convolution_convert_fusion.1 = bf16[512,2048]{1,0:T(8,128)(2,1)} fusion(bf16[2,512,4096]{2,1,0:T(8,128)(2,1)} %constant_dynamic-update-slice_fusion, s32[]{:T(128)S(6)} %select_n.29, bf16[2,2048,512]{2,1,0:T(8,128)(2,1)} %all-gather.8.cloned.1.call-done, bf16[512,512]{1,0:T(8,128)(2,1)} %copy-done.5, bf16[1,512]{1,0:T(2,128)(2,1)S(1)} %collective-permute-done.3, ...), kind=kOutput, calls=%fused_computation.11 | convolution fusion | flops 2157969408 | bytes 8932356 | tf_op jit(solution)/shard_map/dot_general | solution.py:65
  295.1 0.0 all-gather.14.cloned.1.call-start
  295.1 29.8 %reduce-scatter.3.cloned.1.call-done = bf16[512,512]{1,0:T(8,128)(2,1)} async-done(((bf16[512,2048]{1,0:T(8,128)(2,1)}), bf16[512,512]{1,0:T(8,128)(2,1)}) %reduce-scatter.3.cloned.1.call-update) | async-done | bytes 524304 | tf_op jit(solution)/shard_map/reduce_scatter | solution.py:66
  324.9 2.0 add_convert_fusion.1
  326.9 0.0 reduce-scatter.5.cloned.1.call-start
  327.0 22.7 %all-gather.14.cloned.1.call-done = bf16[512,2048]{1,0:T(8,128)(2,1)} async-done(((bf16[512,512]{1,0:T(8,128)(2,1)}), bf16[512,2048]{1,0:T(8,128)(2,1)}) %all-gather.14.cloned.1.call-update) | async-done | bytes 2097168 | tf_op jit(solution)/shard_map/all_gather | solution.py:41
  349.6 2.1 fusion.3
  351.8 3.7 fusion.27
  355.4 0.4 copy-done.6
  355.8 1.3 fusion.28
  357.1 3.4 collective-permute-start.11
  360.5 1.5 collective-permute-start.12
  362.0 4.0 collective-permute-done.12
  366.0 6.3 %convolution_convert_fusion = bf16[512,2048]{1,0:T(8,128)(2,1)} fusion(bf16[2,512,4096]{2,1,0:T(8,128)(2,1)} %constant_dynamic-update-slice_fusion, s32[]{:T(128)S(6)} %add.61, s32[]{:T(128)S(6)} %select_n.29, bf16[2,2048,512]{2,1,0:T(8,128)(2,1)} %all-gather.8.cloned.1.call-done, bf16[512,512]{1,0:T(8,128)(2,1)S(1)} %fusion.28, ...), kind=kOutput, calls=%fused_computation.10 | convolution fusion | flops 2157969408 | bytes 8932360 | tf_op jit(solution)/shard_map/dot_general | solution.py:65
  372.3 31.3 %reduce-scatter.5.cloned.1.call-done = bf16[512,512]{1,0:T(8,128)(2,1)} async-done(((bf16[512,2048]{1,0:T(8,128)(2,1)}), bf16[512,512]{1,0:T(8,128)(2,1)}) %reduce-scatter.5.cloned.1.call-update) | async-done | bytes 524304 | tf_op jit(solution)/shard_map/reduce_scatter | solution.py:66
  403.6 2.0 add_convert_fusion
  (32 shorter events, 0.2 us)
Async XLA Ops:
  6.5 104.9 %copy-start.4 = (bf16[2,512,256]{2,1,0:T(8,128)(2,1)S(1)}, bf16[2,512,256]{2,1,0:T(8,128)(2,1)}, u32[]{:S(2)}) copy-start(bf16[2,512,256]{2,1,0:T(8,128)(2,1)} %param.15) | copy-start | bytes 1572868
  6.5 121.4 %all-gather.6.cloned.1.call-start = ((), (), s32[]{:S(2)}) async-start(), calls=%async_computation.2 | async-start | bytes 2621440 | tf_op jit(solution)/shard_map/all_gather | solution.py:41
  7.3 133.7 %all-gather.12.cloned.1.call-start = ((), (), s32[]{:S(2)}) async-start(), calls=%async_computation.5 | async-start | bytes 4718592 | tf_op jit(solution)/shard_map/all_gather | solution.py:27
  8.0 206.7 %all-gather.10.cloned.1.call-start = ((), (), s32[]{:S(2)}) async-start(), calls=%async_computation.4 | async-start | bytes 4718592 | tf_op jit(solution)/shard_map/all_gather | solution.py:26
  8.7 279.4 %all-gather.8.cloned.1.call-start = ((), (), s32[]{:S(2)}) async-start(), calls=%async_computation.3 | async-start | bytes 4718592 | tf_op jit(solution)/shard_map/all_gather | solution.py:25
  9.3 315.6 %reduce-scatter.3.cloned.1.call-start = ((), (), s32[]{:S(2)}) async-start(), calls=%async_computation.6 | async-start | bytes 2621440 | tf_op jit(solution)/shard_map/reduce_scatter | solution.py:66
  9.4 18.2 %collective-permute-start.4 = (bf16[2,512,256]{2,1,0:T(8,128)(2,1)}, bf16[2,512,256]{2,1,0:T(8,128)(2,1)S(1)}, u32[]{:S(2)}, u32[]{:S(2)}) collective-permute-start(bf16[2,512,256]{2,1,0:T(8,128)(2,1)} %param.15), channel_id=1, source_target_pairs={{0,4},{4,8},{8,12},{12,16},{16,20},{20,24},{24,28},{28,0},{1,5},{5... | collective-permute-start | bytes 1572872 | tf_op jit(solution)/shard_map/ppermute | solution.py:34
  27.6 28.2 %collective-permute-start.5 = (bf16[2,512,256]{2,1,0:T(8,128)(2,1)S(1)}, bf16[2,512,256]{2,1,0:T(8,128)(2,1)S(1)}, u32[]{:S(2)}, u32[]{:S(2)}) collective-permute-start(bf16[2,512,256]{2,1,0:T(8,128)(2,1)S(1)} %collective-permute-done.4), channel_id=1, source_target_pairs={{0,4},{4,8},{8,12},{12,16},{16,20},{20,24},{24,28},{28,0},{1,5},{5... | collective-permute-start | bytes 1572872 | tf_op jit(solution)/shard_map/ppermute | solution.py:34
  27.6 36.6 %collective-permute-start.8 = (bf16[2,512,256]{2,1,0:T(8,128)(2,1)}, bf16[2,512,256]{2,1,0:T(8,128)(2,1)S(1)}, u32[]{:S(2)}, u32[]{:S(2)}) collective-permute-start(bf16[2,512,256]{2,1,0:T(8,128)(2,1)} %param.15), channel_id=1, source_target_pairs={{0,28},{4,0},{8,4},{12,8},{16,12},{20,16},{24,20},{28,24},{1,29},{... | collective-permute-start | bytes 1572872 | tf_op jit(solution)/shard_map/ppermute | solution.py:36
  55.8 22.5 %collective-permute-start.6 = (bf16[2,512,256]{2,1,0:T(8,128)(2,1)S(1)}, bf16[2,512,256]{2,1,0:T(8,128)(2,1)S(1)}, u32[]{:S(2)}, u32[]{:S(2)}) collective-permute-start(bf16[2,512,256]{2,1,0:T(8,128)(2,1)S(1)} %collective-permute-done.5), channel_id=1, source_target_pairs={{0,4},{4,8},{8,12},{12,16},{16,20},{20,24},{24,28},{28,0},{1,5},{5... | collective-permute-start | bytes 1572872 | tf_op jit(solution)/shard_map/ppermute | solution.py:34
  59.6 19.5 %collective-permute-start = (s32[1]{0:T(128)}, s32[1]{0:T(128)}, u32[]{:S(2)}, u32[]{:S(2)}) collective-permute-start(s32[1]{0:T(128)} %get-tuple-element.21), channel_id=1, source_target_pairs={{0,4},{4,8},{8,12},{12,16},{16,20},{20,24},{24,28},{1,5},{5,9},{9,... | collective-permute-start | bytes 20 | tf_op jit(solution)/shard_map/ppermute | solution.py:16
  62.1 17.0 %collective-permute-start.2 = (s32[1]{0:T(128)}, s32[1]{0:T(128)}, u32[]{:S(2)}, u32[]{:S(2)}) collective-permute-start(s32[1]{0:T(128)} %get-tuple-element.22), channel_id=1, source_target_pairs={{4,0},{8,4},{12,8},{16,12},{20,16},{24,20},{28,24},{5,1},{9,5},{13... | collective-permute-start | bytes 20 | tf_op jit(solution)/shard_map/ppermute | solution.py:17
  64.2 32.2 %collective-permute-start.9 = (bf16[2,512,256]{2,1,0:T(8,128)(2,1)S(1)}, bf16[2,512,256]{2,1,0:T(8,128)(2,1)S(1)}, u32[]{:S(2)}, u32[]{:S(2)}) collective-permute-start(bf16[2,512,256]{2,1,0:T(8,128)(2,1)S(1)} %collective-permute-done.8), channel_id=1, source_target_pairs={{0,28},{4,0},{8,4},{12,8},{16,12},{20,16},{24,20},{28,24},{1,29},{... | collective-permute-start | bytes 1572872 | tf_op jit(solution)/shard_map/ppermute | solution.py:36
  78.3 29.6 %collective-permute-start.7 = (bf16[2,512,256]{2,1,0:T(8,128)(2,1)S(1)}, bf16[2,512,256]{2,1,0:T(8,128)(2,1)S(1)}, u32[]{:S(2)}, u32[]{:S(2)}) collective-permute-start(bf16[2,512,256]{2,1,0:T(8,128)(2,1)S(1)} %collective-permute-done.6), channel_id=1, source_target_pairs={{0,4},{4,8},{8,12},{12,16},{16,20},{20,24},{24,28},{28,0},{1,5},{5... | collective-permute-start | bytes 1572872 | tf_op jit(solution)/shard_map/ppermute | solution.py:34
  96.4 24.4 %collective-permute-start.10 = (bf16[2,512,256]{2,1,0:T(8,128)(2,1)S(1)}, bf16[2,512,256]{2,1,0:T(8,128)(2,1)S(1)}, u32[]{:S(2)}, u32[]{:S(2)}) collective-permute-start(bf16[2,512,256]{2,1,0:T(8,128)(2,1)S(1)} %collective-permute-done.9), channel_id=1, source_target_pairs={{0,28},{4,0},{8,4},{12,8},{16,12},{20,16},{24,20},{28,24},{1,29},{... | collective-permute-start | bytes 1572872 | tf_op jit(solution)/shard_map/ppermute | solution.py:36
  140.9 73.8 %copy-start.2 = (bf16[512,2048]{1,0:T(8,128)(2,1)S(1)}, bf16[512,2048]{1,0:T(8,128)(2,1)}, u32[]{:S(2)}) copy-start(bf16[512,2048]{1,0:T(8,128)(2,1)} %all-gather.6.cloned.1.call-done) | copy-start | bytes 6291460
  217.9 3.8 copy-start.5
  217.9 70.2 %collective-permute-start.1 = (bf16[1,512]{1,0:T(2,128)(2,1)S(1)}, bf16[1,512]{1,0:T(2,128)(2,1)S(1)}, u32[]{:S(2)}, u32[]{:S(2)}) collective-permute-start(bf16[1,512]{1,0:T(2,128)(2,1)S(1)} %get-tuple-element.7), channel_id=1, source_target_pairs={{0,4},{4,8},{8,12},{12,16},{16,20},{20,24},{24,28},{1,5},{5,9},{9,... | collective-permute-start | bytes 3080 | tf_op jit(solution)/shard_map/ppermute | solution.py:16
  220.4 67.7 %collective-permute-start.3 = (bf16[1,512]{1,0:T(2,128)(2,1)S(1)}, bf16[1,512]{1,0:T(2,128)(2,1)S(1)}, u32[]{:S(2)}, u32[]{:S(2)}) collective-permute-start(bf16[1,512]{1,0:T(2,128)(2,1)S(1)} %get-tuple-element.8), channel_id=1, source_target_pairs={{4,0},{8,4},{12,8},{16,12},{20,16},{24,20},{28,24},{5,1},{9,5},{13... | collective-permute-start | bytes 3080 | tf_op jit(solution)/shard_map/ppermute | solution.py:17
  288.1 36.8 %copy-start.1 = (bf16[512,512]{1,0:T(8,128)(2,1)S(1)}, bf16[512,512]{1,0:T(8,128)(2,1)}, u32[]{:S(2)}) copy-start(bf16[512,512]{1,0:T(8,128)(2,1)} %param.8) | copy-start | bytes 1572868
  295.1 54.6 %all-gather.14.cloned.1.call-start = ((), (), s32[]{:S(2)}) async-start(), calls=%async_computation.7 | async-start | bytes 2621440 | tf_op jit(solution)/shard_map/all_gather | solution.py:41
  326.9 76.7 %reduce-scatter.5.cloned.1.call-start = ((), (), s32[]{:S(2)}) async-start(), calls=%async_computation.8 | async-start | bytes 2621440 | tf_op jit(solution)/shard_map/reduce_scatter | solution.py:66
  351.7 3.7 copy-start.3
  351.7 4.1 copy-start.6
  357.1 4.9 %collective-permute-start.11 = (bf16[1,512]{1,0:T(2,128)(2,1)S(1)}, bf16[1,512]{1,0:T(2,128)(2,1)S(1)}, u32[]{:S(2)}, u32[]{:S(2)}) collective-permute-start(bf16[1,512]{1,0:T(2,128)(2,1)S(1)} %get-tuple-element.5), channel_id=1, source_target_pairs={{0,4},{4,8},{8,12},{12,16},{16,20},{20,24},{24,28},{1,5},{5,9},{9,... | collective-permute-start | bytes 3080 | tf_op jit(solution)/shard_map/ppermute | solution.py:16
  360.5 5.5 %collective-permute-start.12 = (bf16[1,512]{1,0:T(2,128)(2,1)S(1)}, bf16[1,512]{1,0:T(2,128)(2,1)S(1)}, u32[]{:S(2)}, u32[]{:S(2)}) collective-permute-start(bf16[1,512]{1,0:T(2,128)(2,1)S(1)} %get-tuple-element.6), channel_id=1, source_target_pairs={{4,0},{8,4},{12,8},{16,12},{20,16},{24,20},{28,24},{5,1},{9,5},{13... | collective-permute-start | bytes 3080 | tf_op jit(solution)/shard_map/ppermute | solution.py:17
  366.0 37.6 %copy-start = (bf16[512,512]{1,0:T(8,128)(2,1)S(1)}, bf16[512,512]{1,0:T(8,128)(2,1)}, u32[]{:S(2)}) copy-start(bf16[512,512]{1,0:T(8,128)(2,1)} %add_convert_fusion.1) | copy-start | bytes 1572868
Sparse Core Ops, SparseCore 0:
  8.9 25.2 all-gather.5
  36.4 104.4 all-gather.11
  143.1 71.5 all-gather.9
  216.8 71.2 all-gather.7
  295.2 29.7 reduce-scatter.2
  327.1 22.5 all-gather.13
  372.4 31.1 reduce-scatter.4
